TPU v7x, 512 devices: a whole 4x4x16 slice. The times are simulated.
512 devices in a mesh: fs: 16 (over y, x), tp: 32 (over z, core).
Axes of the slice: x: 4, y: 4, z: 16, core: 2. Of those that a mesh axis runs over, the one named last changes fastest.
Arguments:
- tokens: bfloat16 [16384, 2048], P(('fs', 'tp')), may hold values from -6 to 6
- norm_gain: float32 [2048], P('fs'), may hold values from 0.1 to 1.9
- gate_master: float32 [2048, 8192], P('fs', 'tp'), may hold values from -0.125 to 0.125
- up_master: float32 [2048, 8192], P('fs', 'tp'), may hold values from -0.125 to 0.125
- down_master: float32 [2048, 8192], P('fs', 'tp'), may hold values from -0.125 to 0.125
Outputs:
- mixed: bfloat16 [16384, 2048], P(('fs', 'tp'))
- gate_ready: bfloat16 [2048, 8192], P(None, 'tp')
- up_ready: bfloat16 [2048, 8192], P(None, 'tp')
- down_ready: bfloat16 [2048, 8192], P(None, 'tp')
All inputs are finite; a program needn't handle non-finite values.
Results may differ from a plain program's by a relative error of at most 0.0095.
Values may be sent and summed in bfloat16 or wider, within the bound.
A program may use at most 64 MiB of HBM per device.

v0:
```python
import jax
import jax.numpy as jnp
from jax import lax
from jax.sharding import Mesh
from jax.sharding import PartitionSpec as P

TP = ("tp_0", "tp_1")
FS_TP = ("fs", "tp_0", "tp_1")


def in_one_piece(arrays, axis, dim, along):
    both = jnp.concatenate(arrays, axis=along)
    whole, at, gathered = (lax.all_gather(both, axis, axis=dim, tiled=True), 0, [])
    for a in arrays:
        gathered.append(lax.slice_in_dim(whole, at, at + a.shape[along], axis=along))
        at += a.shape[along]
    return tuple(gathered)


def laid_out(parts, dim):
    dims = list(parts.shape[1:])
    dims[dim] *= parts.shape[0]
    return jnp.moveaxis(parts, 0, dim).reshape(dims)


def copy_for_each(array, axis):
    copies = jnp.broadcast_to(array, (lax.axis_size(axis), *array.shape))
    return lax.all_to_all(copies, axis, split_axis=0, concat_axis=0, tiled=True)


def collect(array, axis, dim):
    return laid_out(copy_for_each(array, axis), dim)


def own_block(parts, axes, sequence):
    inside = parts.shape[1:]
    parts = parts.reshape(*(lax.axis_size(a) for a in axes), *inside)
    parts = jnp.moveaxis(parts, sequence, range(len(axes))).reshape(-1, *inside)
    for k in sequence:
        parts = lax.psum_scatter(parts, axes[k], scatter_dimension=0, tiled=True)
    return parts[0]


def split_up(array, dim, length):
    dims = array.shape
    parts = array.reshape(*dims[:dim], length, dims[dim] // length, *dims[dim + 1 :])
    return jnp.moveaxis(parts, dim, 0)


def sum_by_axis(array, axes, sequence, dim):
    length = lax.axis_size(axes)
    return own_block(split_up(array, dim, length), axes, sequence)


def expand_rows(rows, gate_ready, up_ready):
    rows_wide = rows.astype(jnp.float32)
    row_scale = lax.rsqrt(jnp.mean(rows_wide * rows_wide, axis=1, keepdims=True) + 1e-06)
    gate_proj = row_scale * jnp.dot(rows, gate_ready, preferred_element_type=jnp.float32)
    up_proj = row_scale * jnp.dot(rows, up_ready, preferred_element_type=jnp.float32)
    return (jax.nn.silu(gate_proj) * up_proj).astype(jnp.bfloat16)


def body(tokens, norm_gain, gate_master, up_master, down_master):
    gate_local = (norm_gain[:, None] * gate_master).astype(jnp.bfloat16)
    up_local = (norm_gain[:, None] * up_master).astype(jnp.bfloat16)
    down_local = down_master.astype(jnp.bfloat16)
    gate_ready, up_ready = in_one_piece((gate_local, up_local), "fs", 0, 1)
    gathered = lax.all_gather(tokens, TP, axis=0, tiled=True)
    hidden = expand_rows(gathered, gate_ready, up_ready)
    down_ready = collect(down_local, "fs", 0)
    partial_value = lax.dot_general(
        hidden, down_ready, (((1,), (1,)), ((), ())), preferred_element_type=jnp.float32
    )
    summed = sum_by_axis(partial_value.astype(jnp.bfloat16), TP, (1, 0), 0).astype(jnp.float32)
    mixed = (tokens.astype(jnp.float32) + 0.5 * summed).astype(jnp.bfloat16)
    return (mixed, gate_ready, up_ready, down_ready)


def solution(mesh):
    split = Mesh(mesh.devices.reshape(mesh.shape["fs"], 16, 2), ("fs", "tp_0", "tp_1"))
    placed = (P(FS_TP, None), P("fs"), P("fs", TP), P("fs", TP), P("fs", TP))
    return jax.shard_map(
        body,
        mesh=split,
        in_specs=placed,
        out_specs=(P(FS_TP, None), P(None, TP), P(None, TP), P(None, TP)),
        check_vma=False,
    )
```

profile of v0, /device:TPU:6, one launch (start us, length us, event | category | flops | bytes accessed | tf_op | source)
XLA Modules:
  0.0 275.8 jit_solution(10192223352747149037)
XLA Ops:
  7.2 0.0 all-gather.5.cloned.1.call-start
  7.2 1.1 multiply_convert_fusion.1
  8.3 0.7 pad_maximum_fusion
  9.0 0.0 all-gather.5.cloned.1.call-update
  9.0 0.0 all-gather.3.cloned.1.call-start
  9.0 0.7 all-gather.3.cloned.1.call-update
  9.7 0.9 convert_element_type.33
  10.6 1.1 broadcast_in_dim.2
  11.7 9.3 %all-to-all-start = ((bf16[16,128,256]{2,1,0:T(8,128)(2,1)}), bf16[16,128,256]{2,1,0:T(8,128)(2,1)S(1)}, u32[]{:S(2)}, u32[]{:S(2)}) async-start(bf16[16,128,256]{2,1,0:T(8,128)(2,1)} %broadcast_in_dim.2), calls=%async_computation | async-start | bytes 2097152 | tf_op jit(solution)/shard_map/all_to_all | solution.py:28
  21.0 0.0 reduce-scatter.3.cloned.1.call-start
  21.0 54.8 %all-gather.5.cloned.1.call-done = bf16[2048,512]{1,0:T(8,128)(2,1)} async-done(((bf16[128,512]{1,0:T(8,128)(2,1)}), bf16[2048,512]{1,0:T(8,128)(2,1)}) %all-gather.5.cloned.1.call-update) | async-done | bytes 2097168 | tf_op jit(solution)/shard_map/all_gather | solution.py:13
  75.9 1.7 fusion.13
  77.6 0.0 copy-start.1
  77.6 0.0 copy-start.2
  77.6 73.6 %all-gather.3.cloned.1.call-done = bf16[1024,2048]{1,0:T(8,128)(2,1)} async-done(((bf16[32,2048]{1,0:T(8,128)(2,1)}), bf16[1024,2048]{1,0:T(8,128)(2,1)}) %all-gather.3.cloned.1.call-update) | async-done | bytes 4194320 | tf_op jit(solution)/shard_map/all_gather | solution.py:68
  151.2 0.0 copy-start
  151.2 3.2 %multiply_reduce_fusion = f32[1024]{0:T(1024)S(1)} fusion(bf16[1024,2048]{1,0:T(8,128)(2,1)} %all-gather.3.cloned.1.call-done), kind=kLoop, calls=%fused_computation | loop fusion | flops 6290432 | bytes 4198400 | tf_op jit(solution)/shard_map/reduce_sum | solution.py:57
  154.4 0.2 copy-done
  154.6 2.4 fusion.1
  157.0 0.0 copy-done.1
  157.0 0.0 all-to-all-done
  157.0 0.0 copy-done.2
  157.0 7.0 %convolution_convert_fusion = bf16[1024,2048]{1,0:T(8,128)(2,1)} fusion(bf16[2048,256]{1,0:T(8,128)(2,1)S(1)} %bitcast.26, bf16[2048,256]{1,0:T(8,128)(2,1)S(1)} %get-tuple-element.14, bf16[1024,2048]{1,0:T(8,128)(2,1)} %all-gather.3.cloned.1.call-done, f32[1024,256]{0,1:T(8,128)} %fusion.1, f32[1024]{0:T(1024)S(1)} %add_rsqrt_fusion), kind=kOutput, calls=%fused_computation.1 | convolution fusion | flops 2151415808 | bytes 11538432 | tf_op jit(solution)/shard_map/dot_general | solution.py:71
  164.0 4.7 %copy.9 = bf16[2,16,32,2048]{3,2,1,0:T(8,128)(2,1)} copy(bf16[2,16,32,2048]{3,2,0,1:T(8,128)(2,1)} %bitcast.25) | data formatting | bytes 8388608 | tf_op jit(solution)/shard_map/transpose | solution.py:38
  168.8 0.0 copy-start.3
  168.8 0.0 reduce-scatter.3.cloned.1.call-update
  168.8 0.0 reduce-scatter.5.cloned.1.call-start
  168.9 19.5 %reduce-scatter.3.cloned.1.call-done = bf16[16,32,2048]{2,1,0:T(8,128)(2,1)} async-done(((bf16[32,32,2048]{2,1,0:T(8,128)(2,1)}), bf16[16,32,2048]{2,1,0:T(8,128)(2,1)}) %reduce-scatter.3.cloned.1.call-update) | async-done | bytes 2097168 | tf_op jit(solution)/shard_map/reduce_scatter | solution.py:40
  188.4 0.0 reduce-scatter.5.cloned.1.call-update
  188.4 78.3 %reduce-scatter.5.cloned.1.call-done = bf16[1,32,2048]{2,1,0:T(8,128)(2,1)} async-done(((bf16[16,32,2048]{2,1,0:T(8,128)(2,1)}), bf16[1,32,2048]{2,1,0:T(8,128)(2,1)}) %reduce-scatter.5.cloned.1.call-update) | async-done | bytes 131088 | tf_op jit(solution)/shard_map/reduce_scatter | solution.py:40
  266.7 0.0 copy-done.3
  266.7 1.6 fusion.11
  268.3 1.0 copy.11
  (1 shorter events, 0.0 us)
Async XLA Ops:
  7.2 68.7 %all-gather.5.cloned.1.call-start = ((), (), s32[]{:S(2)}) async-start(), calls=%async_computation.4 | async-start | bytes 2228224 | tf_op jit(solution)/shard_map/all_gather | solution.py:13
  9.0 142.2 %all-gather.3.cloned.1.call-start = ((), (), s32[]{:S(2)}) async-start(), calls=%async_computation.3 | async-start | bytes 4325376 | tf_op jit(solution)/shard_map/all_gather | solution.py:68
  11.7 145.3 %all-to-all-start = ((bf16[16,128,256]{2,1,0:T(8,128)(2,1)}), bf16[16,128,256]{2,1,0:T(8,128)(2,1)S(1)}, u32[]{:S(2)}, u32[]{:S(2)}) async-start(bf16[16,128,256]{2,1,0:T(8,128)(2,1)} %broadcast_in_dim.2), calls=%async_computation | async-start | bytes 2097152 | tf_op jit(solution)/shard_map/all_to_all | solution.py:28
  21.0 167.4 %reduce-scatter.3.cloned.1.call-start = ((), (), s32[]{:S(2)}) async-start(), calls=%async_computation.5 | async-start | bytes 6291456 | tf_op jit(solution)/shard_map/reduce_scatter | solution.py:40
  77.6 79.4 %copy-start.1 = (bf16[2048,256]{1,0:T(8,128)(2,1)}, bf16[2048,256]{1,0:T(8,128)(2,1)S(1)}, u32[]{:S(2)}) copy-start(bf16[2048,256]{1,0:T(8,128)(2,1)S(1)} %get-tuple-element.13) | copy-start | bytes 3145732
  77.6 79.4 %copy-start.2 = (bf16[2048,256]{1,0:T(8,128)(2,1)}, bf16[2048,256]{1,0:T(8,128)(2,1)S(1)}, u32[]{:S(2)}) copy-start(bf16[2048,256]{1,0:T(8,128)(2,1)S(1)} %get-tuple-element.14) | copy-start | bytes 3145732
  151.2 3.4 %copy-start = (bf16[1024,2048]{1,0:T(8,128)(2,1)S(1)}, bf16[1024,2048]{1,0:T(8,128)(2,1)}, u32[]{:S(2)}) copy-start(bf16[1024,2048]{1,0:T(8,128)(2,1)} %all-gather.3.cloned.1.call-done) | copy-start | bytes 12582916
  168.8 97.9 %copy-start.3 = (bf16[32,2048]{1,0:T(8,128)(2,1)S(1)}, bf16[32,2048]{1,0:T(8,128)(2,1)}, u32[]{:S(2)}) copy-start(bf16[32,2048]{1,0:T(8,128)(2,1)} %param.5) | copy-start | bytes 393220
  168.8 97.9 %reduce-scatter.5.cloned.1.call-start = ((), (), s32[]{:S(2)}) async-start(), calls=%async_computation.6 | async-start | bytes 2228224 | tf_op jit(solution)/shard_map/reduce_scatter | solution.py:40
Sparse Core Ops, SparseCore 0:
  11.6 64.2 all-gather.4
  78.0 73.1 all-gather.2
  168.9 19.3 reduce-scatter.2
  191.0 75.5 reduce-scatter.4
where the time goes:
time: 276 us
  waiting for transfers between devices  227 us (82%)
  between operations  13.8 us (5%)
  starting transfers between devices  9.44 us (3%)
  matrix products  9.4 us (3%)
  local copies, waits for them, and re-layouts  8.68 us (3%)
  other arithmetic  7.48 us (3%)
    reduce_scatter x2, waiting for transfers between devices, own_block(): parts = lax.psum_scatter(parts, axes[k], scatter_dimension=0, tiled=True)  97.8 us
    all_gather x1, waiting for transfers between devices, body(): gathered = lax.all_gather(tokens, TP, axis=0, tiled=True)  73.6 us
    all_gather x1, waiting for transfers between devices, in_one_piece(): lax.all_gather(both, axis, axis=dim, tiled=True)  54.8 us
    all_to_all x1, starting transfers between devices, copy_for_each(): return lax.all_to_all(copies, axis, split_axis=0, concat_axis=0, tiled=True)  9.28 us
    dot_general x1, matrix products, body(): lax.dot_general(hidden, down_ready, (((1,), (1,)), ((), ())), preferred_e...  7.04 us
  transfers between devices with their start and end apart: 5, of which 4 were waited for; matrix products, arithmetic and copies ran while one was open for 3% of the time, Pallas kernels for 0%

commit v1 on v0

--- a/solution.py
+++ b/solution.py
@@ -65,7 +65,9 @@
     up_local = (norm_gain[:, None] * up_master).astype(jnp.bfloat16)
     down_local = down_master.astype(jnp.bfloat16)
     gate_ready, up_ready = in_one_piece((gate_local, up_local), "fs", 0, 1)
-    gathered = lax.all_gather(tokens, TP, axis=0, tiled=True)
+    gathered = jnp.concatenate(
+        lax.all_to_all(jnp.stack([tokens] * lax.axis_size(TP)), TP, 0, 0), axis=0
+    )
     hidden = expand_rows(gathered, gate_ready, up_ready)
     down_ready = collect(down_local, "fs", 0)
     partial_value = lax.dot_general(

time: 276 us -> 353 us (1.28)
  waiting for transfers between devices: 227 us -> 286 us
  starting transfers between devices: 9.44 us -> 23.3 us
    all_to_all x0 -> x1, waiting for transfers between devices: none -> 116 us  [body(): lax.all_to_all(jnp.stack([tokens] * lax.axis_size(TP)), TP, 0, 0)]
    all_gather x1 -> x0, waiting for transfers between devices: 73.6 us -> none  [body(): gathered = lax.all_gather(tokens, TP, axis=0, tiled=True)]
    all_to_all x0 -> x1, starting transfers between devices: none -> 15.8 us  [body(): lax.all_to_all(jnp.stack([tokens] * lax.axis_size(TP)), TP, 0, 0)]
    all_gather x1, waiting for transfers between devices: 54.8 us -> 64.5 us  [in_one_piece(): lax.all_gather(both, axis, axis=dim, tiled=True)]
    all_to_all x1, waiting for transfers between devices: 0.01 us -> 6.99 us  [copy_for_each(): return lax.all_to_all(copies, axis, split_axis=0, concat_axis=0, tiled=True)]
  transfers between devices with their start and end apart: 5 -> 5, of which waited for: 4 -> 5; matrix products, arithmetic and copies ran while one was open for 3% -> 3% of each run, Pallas kernels for 0% -> 0%
where the time goes in v1:
time: 353 us
  waiting for transfers between devices  286 us (81%)
  starting transfers between devices  23.3 us (7%)
  between operations  13.8 us (4%)
  local copies, waits for them, and re-layouts  11.9 us (3%)
  matrix products  11.6 us (3%)
  other arithmetic  5.44 us (2%)
    all_to_all x1, waiting for transfers between devices, body(): lax.all_to_all(jnp.stack([tokens] * lax.axis_size(TP)), TP, 0, 0)  116 us
    reduce_scatter x2, waiting for transfers between devices, own_block(): parts = lax.psum_scatter(parts, axes[k], scatter_dimension=0, tiled=True)  98.5 us
    all_gather x1, waiting for transfers between devices, in_one_piece(): lax.all_gather(both, axis, axis=dim, tiled=True)  64.5 us
    all_to_all x1, starting transfers between devices, body(): lax.all_to_all(jnp.stack([tokens] * lax.axis_size(TP)), TP, 0, 0)  15.8 us
    all_to_all x1, starting transfers between devices, copy_for_each(): return lax.all_to_all(copies, axis, split_axis=0, concat_axis=0, tiled=True)  7.42 us
  transfers between devices with their start and end apart: 5, of which 5 were waited for; matrix products, arithmetic and copies ran while one was open for 3% of the time, Pallas kernels for 0%

profile of v1, /device:TPU:6, one launch (start us, length us, event | category | flops | bytes accessed | tf_op | source)
XLA Modules:
  0.0 352.6 jit_solution(9775286297000736503)
XLA Ops:
  7.2 3.4 stack.2
  10.6 0.0 copy-start.4
  10.6 0.0 copy-start.5
  10.6 0.0 copy-start.6
  10.6 0.0 copy-start.3
  10.6 15.8 %all-to-all-start = ((bf16[32,32,2048]{2,1,0:T(8,128)(2,1)}), bf16[32,32,2048]{2,1,0:T(8,128)(2,1)}, u32[]{:S(2)}, u32[]{:S(2)}) async-start(bf16[32,32,2048]{2,1,0:T(8,128)(2,1)} %stack.2), calls=%async_computation | async-start | bytes 8388608 | tf_op jit(solution)/shard_map/all_to_all | solution.py:69
  26.3 0.0 all-gather.2.cloned.1.call-start
  26.4 0.0 copy-done.4
  26.4 0.0 copy-done.5
  26.4 0.0 copy-done.6
  26.4 0.1 multiply_convert_fusion.1
  26.5 0.7 pad_maximum_fusion
  27.2 0.0 all-gather.2.cloned.1.call-update
  27.2 0.0 copy-done.3
  27.2 64.5 %all-gather.2.cloned.1.call-done = bf16[2048,512]{1,0:T(8,128)(2,1)} async-done(((bf16[128,512]{1,0:T(8,128)(2,1)}), bf16[2048,512]{1,0:T(8,128)(2,1)}) %all-gather.2.cloned.1.call-update) | async-done | bytes 2097168 | tf_op jit(solution)/shard_map/all_gather | solution.py:13
  91.7 1.7 fusion.13
  93.4 0.0 copy-start
  93.4 0.0 copy-start.1
  93.4 116.4 %all-to-all-done = bf16[32,32,2048]{2,1,0:T(8,128)(2,1)} async-done(((bf16[32,32,2048]{2,1,0:T(8,128)(2,1)}), bf16[32,32,2048]{2,1,0:T(8,128)(2,1)}, u32[]{:S(2)}, u32[]{:S(2)}) %all-to-all-start) | async-done | bytes 4194336 | tf_op jit(solution)/shard_map/all_to_all | solution.py:69
  209.8 1.1 broadcast_in_dim.2
  210.9 7.4 %all-to-all-start.1 = ((bf16[16,128,256]{2,1,0:T(8,128)(2,1)}), bf16[16,128,256]{2,1,0:T(8,128)(2,1)S(1)}, u32[]{:S(2)}, u32[]{:S(2)}) async-start(bf16[16,128,256]{2,1,0:T(8,128)(2,1)} %broadcast_in_dim.2), calls=%async_computation.1 | async-start | bytes 2097152 | tf_op jit(solution)/shard_map/all_to_all | solution.py:28
  218.3 0.0 reduce-scatter.3.cloned.1.call-start
  218.4 3.1 multiply_reduce_fusion
  221.5 0.1 rsqrt.12
  221.5 4.6 %fusion.1 = f32[1024,256]{0,1:T(8,128)} fusion(bf16[2048,256]{1,0:T(8,128)(2,1)S(1)} %get-tuple-element.13, bf16[1024,2048]{1,0:T(8,128)(2,1)} %bitcast, f32[1024]{0:T(1024)S(1)} %rsqrt.12), kind=kOutput, calls=%fused_computation.5 | convolution fusion | flops 1074003968 | bytes 6295552 | tf_op jit(solution)/shard_map/dot_general | solution.py:58
  226.1 0.0 copy-done
  226.1 7.0 %all-to-all-done.1 = bf16[16,128,256]{2,1,0:T(8,128)(2,1)S(1)} async-done(((bf16[16,128,256]{2,1,0:T(8,128)(2,1)}), bf16[16,128,256]{2,1,0:T(8,128)(2,1)S(1)}, u32[]{:S(2)}, u32[]{:S(2)}) %all-to-all-start.1) | async-done | bytes 1048608 | tf_op jit(solution)/shard_map/all_to_all | solution.py:28
  233.1 0.0 copy-done.1
  233.1 7.0 %convolution_convert_fusion = bf16[1024,2048]{1,0:T(8,128)(2,1)} fusion(bf16[2048,256]{1,0:T(8,128)(2,1)S(1)} %bitcast.27, bf16[2048,256]{1,0:T(8,128)(2,1)S(1)} %get-tuple-element.14, bf16[1024,2048]{1,0:T(8,128)(2,1)} %bitcast, f32[1024,256]{0,1:T(8,128)} %fusion.1, f32[1024]{0:T(1024)S(1)} %rsqrt.12), kind=kOutput, calls=%fused_computation.1 | convolution fusion | flops 2151415808 | bytes 11538432 | tf_op jit(solution)/shard_map/dot_general | solution.py:73
  240.1 4.7 %copy.10 = bf16[2,16,32,2048]{3,2,1,0:T(8,128)(2,1)} copy(bf16[2,16,32,2048]{3,2,0,1:T(8,128)(2,1)} %bitcast.26) | data formatting | bytes 8388608 | tf_op jit(solution)/shard_map/transpose | solution.py:38
  244.9 0.0 copy-start.2
  244.9 0.0 reduce-scatter.3.cloned.1.call-update
  244.9 0.0 reduce-scatter.5.cloned.1.call-start
  244.9 20.0 %reduce-scatter.3.cloned.1.call-done = bf16[16,32,2048]{2,1,0:T(8,128)(2,1)} async-done(((bf16[32,32,2048]{2,1,0:T(8,128)(2,1)}), bf16[16,32,2048]{2,1,0:T(8,128)(2,1)}) %reduce-scatter.3.cloned.1.call-update) | async-done | bytes 2097168 | tf_op jit(solution)/shard_map/reduce_scatter | solution.py:40
  265.0 0.0 reduce-scatter.5.cloned.1.call-update
  265.0 78.5 %reduce-scatter.5.cloned.1.call-done = bf16[1,32,2048]{2,1,0:T(8,128)(2,1)} async-done(((bf16[16,32,2048]{2,1,0:T(8,128)(2,1)}), bf16[1,32,2048]{2,1,0:T(8,128)(2,1)}) %reduce-scatter.5.cloned.1.call-update) | async-done | bytes 131088 | tf_op jit(solution)/shard_map/reduce_scatter | solution.py:40
  343.5 0.0 copy-done.2
  343.5 1.6 fusion.11
  345.1 1.0 copy.12
  (2 shorter events, 0.0 us)
Async XLA Ops:
  10.6 15.8 %copy-start.4 = (f32[128,256]{1,0:T(8,128)S(1)}, f32[128,256]{1,0:T(8,128)}, u32[]{:S(2)}) copy-start(f32[128,256]{1,0:T(8,128)} %param.7) | copy-start | bytes 393220
  10.6 15.8 %copy-start.5 = (f32[128,256]{1,0:T(8,128)S(1)}, f32[128,256]{1,0:T(8,128)}, u32[]{:S(2)}) copy-start(f32[128,256]{1,0:T(8,128)} %param.8) | copy-start | bytes 393220
  10.6 15.8 %copy-start.6 = (f32[128]{0:T(128)S(1)}, f32[128]{0:T(128)}, u32[]{:S(2)}) copy-start(f32[128]{0:T(128)} %param.6) | copy-start | bytes 1540
  10.6 16.6 %copy-start.3 = (f32[128,256]{1,0:T(8,128)S(1)}, f32[128,256]{1,0:T(8,128)}, u32[]{:S(2)}) copy-start(f32[128,256]{1,0:T(8,128)} %param.9) | copy-start | bytes 393220
  10.6 199.3 %all-to-all-start = ((bf16[32,32,2048]{2,1,0:T(8,128)(2,1)}), bf16[32,32,2048]{2,1,0:T(8,128)(2,1)}, u32[]{:S(2)}, u32[]{:S(2)}) async-start(bf16[32,32,2048]{2,1,0:T(8,128)(2,1)} %stack.2), calls=%async_computation | async-start | bytes 8388608 | tf_op jit(solution)/shard_map/all_to_all | solution.py:69
  26.3 65.3 %all-gather.2.cloned.1.call-start = ((), (), s32[]{:S(2)}) async-start(), calls=%async_computation.4 | async-start | bytes 2228224 | tf_op jit(solution)/shard_map/all_gather | solution.py:13
  93.4 132.7 %copy-start = (bf16[2048,256]{1,0:T(8,128)(2,1)}, bf16[2048,256]{1,0:T(8,128)(2,1)S(1)}, u32[]{:S(2)}) copy-start(bf16[2048,256]{1,0:T(8,128)(2,1)S(1)} %get-tuple-element.13) | copy-start | bytes 3145732
  93.4 139.7 %copy-start.1 = (bf16[2048,256]{1,0:T(8,128)(2,1)}, bf16[2048,256]{1,0:T(8,128)(2,1)S(1)}, u32[]{:S(2)}) copy-start(bf16[2048,256]{1,0:T(8,128)(2,1)S(1)} %get-tuple-element.14) | copy-start | bytes 3145732
  210.9 22.2 %all-to-all-start.1 = ((bf16[16,128,256]{2,1,0:T(8,128)(2,1)}), bf16[16,128,256]{2,1,0:T(8,128)(2,1)S(1)}, u32[]{:S(2)}, u32[]{:S(2)}) async-start(bf16[16,128,256]{2,1,0:T(8,128)(2,1)} %broadcast_in_dim.2), calls=%async_computation.1 | async-start | bytes 2097152 | tf_op jit(solution)/shard_map/all_to_all | solution.py:28
  218.3 46.6 %reduce-scatter.3.cloned.1.call-start = ((), (), s32[]{:S(2)}) async-start(), calls=%async_computation.5 | async-start | bytes 6291456 | tf_op jit(solution)/shard_map/reduce_scatter | solution.py:40
  244.9 98.6 %copy-start.2 = (bf16[32,2048]{1,0:T(8,128)(2,1)S(1)}, bf16[32,2048]{1,0:T(8,128)(2,1)}, u32[]{:S(2)}) copy-start(bf16[32,2048]{1,0:T(8,128)(2,1)} %param.5) | copy-start | bytes 393220
  244.9 98.6 %reduce-scatter.5.cloned.1.call-start = ((), (), s32[]{:S(2)}) async-start(), calls=%async_computation.6 | async-start | bytes 2228224 | tf_op jit(solution)/shard_map/reduce_scatter | solution.py:40
Sparse Core Ops, SparseCore 0:
  30.7 60.9 all-gather.1
  245.0 19.9 reduce-scatter.2
  267.8 75.6 reduce-scatter.4
